TPU v7x, 32 devices: a whole 2x2x4 slice. The times are simulated.
32 devices in a mesh: sp: 8 (over z, x), dp: 4 (over y, core).
Axes of the slice: x: 2, y: 2, z: 4, core: 2. Of those that a mesh axis runs over, the one named last changes fastest.
Arguments:
- tokens: bfloat16 [32, 512, 2048], P('dp', 'sp'), may hold values from -6 to 6
- pre_gain: float32 [2048], replicated, may hold values from 0.1 to 1.9
- w_query: bfloat16 [2048, 512], P('dp'), may hold values from -0.125 to 0.125
- w_forget: bfloat16 [2048, 512], P('dp'), may hold values from -0.125 to 0.125
- w_value: bfloat16 [2048, 512], P('dp'), may hold values from -0.125 to 0.125
- w_gate: bfloat16 [2048, 512], P('dp'), may hold values from -0.125 to 0.125
- lower_bound: float32 [512], replicated, may hold values from 0.8 to 1
- extra_decay: float32 [128, 512], P(('dp', 'sp')), may hold values from -1.5 to 0
- initial_state: float32 [128, 128, 128], P(('dp', 'sp')), may hold values from -0.18 to 0.18
- norm_gain: float32 [128], replicated, may hold values from 0.1 to 1.9
- w_out: bfloat16 [512, 2048], P('dp'), may hold values from -0.25 to 0.25
- post_gain: float32 [2048], replicated, may hold values from 0.1 to 1.9
Outputs:
- layer_out: bfloat16 [32, 512, 2048], P('dp', 'sp')
All inputs are finite; a program needn't handle non-finite values.
Results may differ from a plain program's by a relative error of at most 0.015.
Values may be sent and summed in bfloat16 or wider, within the bound.
A program may use at most 64 MiB of HBM per device.

v0:
```python
import jax
import jax.numpy as jnp
from jax import lax
from jax.sharding import PartitionSpec as P

HEADS = 4
HK = 128
HV = 128
BLOCK = 64


EPS = 1e-06


def rms_scale(matrix, gain):
    widened = matrix.astype(jnp.float32)
    return widened * lax.rsqrt(jnp.mean(widened * widened, axis=-1, keepdims=True) + EPS) * gain


def recur_item(queries, keys_in, values, log_decay, state_zero):
    length = queries.shape[0]
    block_count = length // BLOCK

    def blocks(matrix):
        return matrix.reshape(block_count, BLOCK, matrix.shape[-1])

    causal_mask = jnp.tril(jnp.ones((BLOCK, BLOCK), dtype=bool))

    def block_step(carried_state, inputs):
        query_block, key_block, value_block, decay_block = inputs
        cumulative = jnp.cumsum(decay_block, axis=0)
        query_scaled = query_block * jnp.exp(cumulative)
        carried = jnp.dot(query_scaled, carried_state, precision=lax.Precision.HIGHEST)
        key_scaled = key_block * jnp.exp(-cumulative)
        scores = jnp.where(
            causal_mask, jnp.dot(query_scaled, key_scaled.T, precision=lax.Precision.HIGHEST), 0.0
        )
        within = jnp.dot(scores, value_block, precision=lax.Precision.HIGHEST)
        block_end = cumulative[-1]
        added_state = jnp.dot(
            (key_block * jnp.exp(block_end[None, :] - cumulative)).T,
            value_block,
            precision=lax.Precision.HIGHEST,
        )
        return (jnp.exp(block_end)[:, None] * carried_state + added_state, carried + within)

    _, block_outs = lax.scan(
        block_step,
        state_zero,
        (blocks(queries), blocks(keys_in), blocks(values), blocks(log_decay)),
    )
    return block_outs.reshape(length, values.shape[-1])


def normed_heads(q_pre, f_pre, v_pre, forget_gap, extra_rows, state_zero, norm_gain):
    queries = jax.nn.silu(q_pre.astype(jnp.float32))
    keys_in = forget_gap[:, None, :] * jax.nn.sigmoid(-f_pre.astype(jnp.float32))
    log_decay = jnp.log1p(-keys_in) + extra_rows[:, :, None]
    values = v_pre.astype(jnp.float32)
    outputs = jax.vmap(recur_item)(queries, keys_in, values, log_decay, state_zero)
    scaled = (
        outputs * lax.rsqrt(jnp.mean(outputs * outputs, axis=-1, keepdims=True) + EPS) * norm_gain
    )
    return scaled.astype(jnp.bfloat16)


def apply_gate(head_normed, g_pre):
    held = lax.optimization_barrier(head_normed)
    return (held.astype(jnp.float32) * jax.nn.silu(g_pre.astype(jnp.float32))).astype(jnp.bfloat16)


def project(norm_result, weight_in):
    reshaped_input = weight_in.reshape(weight_in.shape[0], HEADS, weight_in.shape[1] // HEADS)
    return jnp.einsum(
        "jbq,qom->jobm", norm_result, reshaped_input, preferred_element_type=jnp.float32
    )


def body(
    tokens,
    pre_gain,
    w_query,
    w_forget,
    w_value,
    w_gate,
    lower_bound,
    extra_decay,
    initial_state,
    norm_gain,
    w_out,
    post_gain,
):
    seq_count, local_len, width = tokens.shape
    norm_result = rms_scale(tokens, pre_gain).astype(jnp.bfloat16)
    columns = norm_result
    q_sum = project(columns, lax.all_gather(w_query, "dp", axis=0, tiled=True))
    f_sum = project(columns, lax.all_gather(w_forget, "dp", axis=0, tiled=True))
    v_sum = project(columns, lax.all_gather(w_value, "dp", axis=0, tiled=True))
    g_sum = project(columns, lax.all_gather(w_gate, "dp", axis=0, tiled=True))
    item_shape = (seq_count * HEADS, local_len, HK)
    gate_local = g_sum.astype(jnp.bfloat16)
    q_pre, f_pre, v_pre = (
        lax.all_to_all(
            q_sum.astype(jnp.bfloat16).reshape(item_shape),
            "sp",
            split_axis=0,
            concat_axis=1,
            tiled=True,
        ),
        lax.all_to_all(
            f_sum.astype(jnp.bfloat16).reshape(item_shape),
            "sp",
            split_axis=0,
            concat_axis=1,
            tiled=True,
        ),
        lax.all_to_all(
            v_sum.astype(jnp.bfloat16).reshape(item_shape),
            "sp",
            split_axis=0,
            concat_axis=1,
            tiled=True,
        ),
    )
    item_count = q_pre.shape[0]
    first_item = lax.axis_index("sp") * item_count
    head_index = (first_item + jnp.arange(item_count, dtype=jnp.int32)) % HEADS
    head_onehot = (head_index[:, None] == jnp.arange(HEADS, dtype=jnp.int32)[None, :]).astype(
        jnp.float32
    )
    forget_gap = jnp.dot(
        head_onehot, (1.0 - lower_bound).reshape(HEADS, HK), precision=lax.Precision.HIGHEST
    )
    head_normed = normed_heads(
        q_pre, f_pre, v_pre, forget_gap, extra_decay, initial_state, norm_gain
    )
    returned = lax.all_to_all(head_normed, "sp", split_axis=1, concat_axis=0, tiled=True)
    by_token = (
        returned.reshape(seq_count, HEADS, local_len, HV)
        .transpose(0, 2, 1, 3)
        .reshape(seq_count * local_len, HEADS * HV)
    )
    gate_rows_local = gate_local.transpose(0, 2, 1, 3).reshape(seq_count * local_len, HEADS * HV)
    by_token = apply_gate(by_token, gate_rows_local)
    columns = by_token
    mixed = jnp.dot(
        columns, lax.all_gather(w_out, "dp", axis=0, tiled=True), preferred_element_type=jnp.float32
    )
    return rms_scale(mixed, post_gain).astype(jnp.bfloat16).reshape(seq_count, local_len, width)


def solution(mesh):
    in_specs = (
        P("dp", "sp", None),
        P(),
        P("dp", None),
        P("dp", None),
        P("dp", None),
        P("dp", None),
        P(),
        P(("dp", "sp"), None),
        P(("dp", "sp"), None, None),
        P(),
        P("dp", None),
        P(),
    )
    out_specs = P("dp", "sp", None)
    return jax.shard_map(body, mesh=mesh, in_specs=in_specs, out_specs=out_specs, check_vma=False)
```

profile of v0, /device:TPU:0, one launch (start us, length us, event | category | flops | bytes accessed | tf_op | source)
XLA Modules:
  0.0 186.1 jit_solution(10344705522578712323)
XLA Ops:
  6.5 2.1 %copy.29 = bf16[512,512]{0,1:T(8,128)(2,1)} copy(bf16[512,512]{1,0:T(8,128)(2,1)} %param.18) | data formatting | bytes 1048576 | tf_op args[4]
  8.8 1.0 copy.31
  10.9 2.1 %copy.35 = bf16[512,512]{0,1:T(8,128)(2,1)} copy(bf16[512,512]{1,0:T(8,128)(2,1)} %param.19) | data formatting | bytes 1048576 | tf_op args[5]
  13.6 20.6 %all-gather.8.cloned.1.call-done = bf16[2048,512]{0,1:T(8,128)(2,1)} async-done(((bf16[512,512]{0,1:T(8,128)(2,1)}), bf16[2048,512]{0,1:T(8,128)(2,1)}) %all-gather.8.cloned.1.call-update) | async-done | bytes 2097168 | tf_op jit(solution)/shard_map/all_gather | solution.py:98
  34.2 3.7 %convolution_convert_fusion.2 = bf16[8,64,4,128]{3,1,2,0:T(8,128)(2,1)} fusion(bf16[2048,4,128,1]{0,2,1,3:T(8,128)(2,1)} %bitcast.145, bf16[8,64,2048]{2,1,0:T(8,128)(2,1)S(1)} %copy-done.1, f32[2048]{0:T(1024)S(1)} %copy-done.8, f32[8,64]{1,0:T(8,128)S(1)} %add_rsqrt_fusion.1), kind=kOutput, calls=%fused_computation.40 | convolution fusion | flops 1078198272 | bytes 4728832 | tf_op jit(solution)/shard_map/jbq,qom->jobm/dot_general | solution.py:74
  37.9 5.5 %all-to-all-start.1 = ((bf16[32,64,128]{2,1,0:T(8,128)(2,1)}), bf16[32,64,128]{2,1,0:T(8,128)(2,1)S(1)}, u32[]{:S(2)}, u32[]{:S(2)}) async-start(bf16[32,64,128]{2,1,0:T(8,128)(2,1)} %bitcast.13), calls=%async_computation.1 | async-start | bytes 1048576 | tf_op jit(solution)/shard_map/all_to_all | solution.py:117
  43.4 14.9 %all-gather.10.cloned.1.call-done = bf16[2048,512]{0,1:T(8,128)(2,1)} async-done(((bf16[512,512]{0,1:T(8,128)(2,1)}), bf16[2048,512]{0,1:T(8,128)(2,1)}) %all-gather.10.cloned.1.call-update) | async-done | bytes 2097168 | tf_op jit(solution)/shard_map/all_gather | solution.py:96
  58.4 3.7 %convolution_convert_fusion.1 = bf16[8,64,4,128]{3,1,2,0:T(8,128)(2,1)} fusion(bf16[2048,4,128,1]{0,2,1,3:T(8,128)(2,1)} %bitcast.146, bf16[8,64,2048]{2,1,0:T(8,128)(2,1)S(1)} %copy-done.1, f32[2048]{0:T(1024)S(1)} %copy-done.8, f32[8,64]{1,0:T(8,128)S(1)} %add_rsqrt_fusion.1), kind=kOutput, calls=%fused_computation.39 | convolution fusion | flops 1078198272 | bytes 4728832 | tf_op jit(solution)/shard_map/jbq,qom->jobm/dot_general | solution.py:74
  62.1 5.5 %all-to-all-start.2 = ((bf16[32,64,128]{2,1,0:T(8,128)(2,1)}), bf16[32,64,128]{2,1,0:T(8,128)(2,1)S(1)}, u32[]{:S(2)}, u32[]{:S(2)}) async-start(bf16[32,64,128]{2,1,0:T(8,128)(2,1)} %bitcast.138), calls=%async_computation.2 | async-start | bytes 1048576 | tf_op jit(solution)/shard_map/all_to_all | solution.py:103
  67.6 15.0 %all-gather.6.cloned.1.call-done = bf16[2048,512]{0,1:T(8,128)(2,1)} async-done(((bf16[512,512]{0,1:T(8,128)(2,1)}), bf16[2048,512]{0,1:T(8,128)(2,1)}) %all-gather.6.cloned.1.call-update) | async-done | bytes 2097168 | tf_op jit(solution)/shard_map/all_gather | solution.py:97
  82.5 3.7 %convolution_convert_fusion.3 = bf16[8,64,4,128]{3,1,2,0:T(8,128)(2,1)} fusion(bf16[2048,4,128,1]{0,2,1,3:T(8,128)(2,1)} %bitcast.144, bf16[8,64,2048]{2,1,0:T(8,128)(2,1)S(1)} %copy-done.1, f32[2048]{0:T(1024)S(1)} %copy-done.8, f32[8,64]{1,0:T(8,128)S(1)} %add_rsqrt_fusion.1), kind=kOutput, calls=%fused_computation.41 | convolution fusion | flops 1078198272 | bytes 4728832 | tf_op jit(solution)/shard_map/jbq,qom->jobm/dot_general | solution.py:74
  86.3 5.5 %all-to-all-start = ((bf16[32,64,128]{2,1,0:T(8,128)(2,1)}), bf16[32,64,128]{2,1,0:T(8,128)(2,1)}, u32[]{:S(2)}, u32[]{:S(2)}) async-start(bf16[32,64,128]{2,1,0:T(8,128)(2,1)} %bitcast.137), calls=%async_computation | async-start | bytes 1048576 | tf_op jit(solution)/shard_map/all_to_all | solution.py:110
  93.1 13.7 %all-to-all-done = bf16[32,64,128]{2,1,0:T(8,128)(2,1)} async-done(((bf16[32,64,128]{2,1,0:T(8,128)(2,1)}), bf16[32,64,128]{2,1,0:T(8,128)(2,1)}, u32[]{:S(2)}, u32[]{:S(2)}) %all-to-all-start) | async-done | bytes 524320 | tf_op jit(solution)/shard_map/all_to_all | solution.py:110
  106.8 1.3 add_divide_fusion
  108.1 1.8 log-plus-one_add_fusion
  109.8 42.0 %while.13 = (s32[]{:T(128)}, f32[4,128,128]{2,1,0:T(8,128)S(1)}, f32[8,4,64,128]{3,2,0,1:T(8,128)}, f32[8,4,64,128]{3,2,1,0:T(8,128)}, f32[8,4,64,128]{3,2,1,0:T...) while((s32[]{:T(128)}, f32[4,128,128]{2,1,0:T(8,128)S(1)}, ...), condition=%wide.region_3.4_spmd.clone, body=%wide.region_1.3_spmd.clone.sunk | while | flops 153440256 | bytes 3239017 | solution.py:47
  110.9 1.3 convolution_select_fusion.2
  112.5 1.0 fusion.69
  113.5 1.6 convolution_add_fusion.3
  116.2 1.3 convolution_select_fusion.2
  117.7 1.0 fusion.69
  118.8 1.6 convolution_add_fusion.3
  121.4 1.3 convolution_select_fusion.2
  123.0 1.0 fusion.69
  124.0 1.6 convolution_add_fusion.3
  126.7 1.3 convolution_select_fusion.2
  128.2 1.0 fusion.69
  129.3 1.6 convolution_add_fusion.3
  131.9 1.3 convolution_select_fusion.2
  133.5 1.0 fusion.69
  134.5 1.6 convolution_add_fusion.3
  137.2 1.3 convolution_select_fusion.2
  138.7 1.0 fusion.69
  139.8 1.6 convolution_add_fusion.3
  142.4 1.3 convolution_select_fusion.2
  144.0 1.0 fusion.69
  145.0 1.6 convolution_add_fusion.3
  147.7 1.3 convolution_select_fusion.2
  149.2 1.0 fusion.69
  150.3 1.6 convolution_add_fusion.3
  151.9 1.6 fusion.34
  153.5 1.7 fusion.33
  155.2 1.2 copy.34
  156.4 3.7 %all-to-all-start.3 = ((bf16[4,512,128]{2,0,1:T(4,128)(2,1)}), bf16[4,512,128]{2,0,1:T(4,128)(2,1)S(1)}, u32[]{:S(2)}, u32[]{:S(2)}) async-start(bf16[4,512,128]{2,0,1:T(4,128)(2,1)} %copy.34), calls=%async_computation.3 | async-start | bytes 1048576 | tf_op jit(solution)/shard_map/all_to_all | solution.py:137
  160.2 2.9 %fusion.24 = f32[8,64,4,128]{3,1,2,0:T(8,128)S(1)} fusion(bf16[2048,4,128,1]{0,2,1,3:T(8,128)(2,1)} %bitcast.143, bf16[8,64,2048]{2,1,0:T(8,128)(2,1)S(1)} %copy-done.2, f32[2048]{0:T(1024)S(1)} %copy-done.8, f32[8,64]{1,0:T(8,128)S(1)} %add_rsqrt_fusion.1), kind=kOutput, calls=%fused_computation.38 | convolution fusion | flops 1078460416 | bytes 5253120 | tf_op jit(solution)/shard_map/jbq,qom->jobm/dot_general | solution.py:74
  163.7 11.0 %all-to-all-done.3 = bf16[4,512,128]{2,0,1:T(4,128)(2,1)S(1)} async-done(((bf16[4,512,128]{2,0,1:T(4,128)(2,1)}), bf16[4,512,128]{2,0,1:T(4,128)(2,1)S(1)}, u32[]{:S(2)}, u32[]{:S(2)}) %all-to-all-start.3) | async-done | bytes 524320 | tf_op jit(solution)/shard_map/all_to_all | solution.py:137
  174.9 3.0 %multiply_reduce_fusion = (f32[512]{0:T(512)S(1)}, f32[512,2048]{1,0:T(8,128)S(1)}) fusion(bf16[512,2048]{1,0:T(8,128)(2,1)} %all-gather.14.cloned.1.call-done, f32[64,8,4,128]{3,2,1,0:T(4,128)S(1)} %bitcast.136, bf16[512,512]{1,0:T(8,128)(2,1)S(1)} %bitcast.139), kind=kOutput, calls=%fused_computation.33 | convolution fusion | flops 1077673472 | bytes 7866368 | tf_op jit(solution)/shard_map/dot_general | solution.py:146
  177.9 1.7 multiply_convert_fusion
  (97 shorter events, 14.6 us)
Async XLA Ops:
  6.5 2.2 %copy-start.3 = (bf16[512,512]{1,0:T(8,128)(2,1)S(1)}, bf16[512,512]{1,0:T(8,128)(2,1)}, u32[]{:S(2)}) copy-start(bf16[512,512]{1,0:T(8,128)(2,1)} %param.16) | copy-start | bytes 1572868
  6.5 3.3 %copy-start.4 = (bf16[512,512]{1,0:T(8,128)(2,1)S(1)}, bf16[512,512]{1,0:T(8,128)(2,1)}, u32[]{:S(2)}) copy-start(bf16[512,512]{1,0:T(8,128)(2,1)} %param.17) | copy-start | bytes 1572868
  6.5 27.7 %all-gather.8.cloned.1.call-start = ((), (), s32[]{:S(2)}) async-start(), calls=%async_computation.5 | async-start | bytes 2621440 | tf_op jit(solution)/shard_map/all_gather | solution.py:98
  8.7 49.7 %all-gather.10.cloned.1.call-start = ((), (), s32[]{:S(2)}) async-start(), calls=%async_computation.6 | async-start | bytes 2621440 | tf_op jit(solution)/shard_map/all_gather | solution.py:96
  9.8 3.3 %copy-start.1 = (bf16[8,64,2048]{2,1,0:T(8,128)(2,1)S(1)}, bf16[8,64,2048]{2,1,0:T(8,128)(2,1)}, u32[]{:S(2)}) copy-start(bf16[8,64,2048]{2,1,0:T(8,128)(2,1)} %param.14) | copy-start | bytes 6291460
  9.8 72.7 %all-gather.6.cloned.1.call-start = ((), (), s32[]{:S(2)}) async-start(), calls=%async_computation.4 | async-start | bytes 2621440 | tf_op jit(solution)/shard_map/all_gather | solution.py:97
  10.9 23.4 %copy-start.8 = (f32[2048]{0:T(1024)S(1)}, f32[2048]{0:T(1024)}, u32[]{:S(2)}) copy-start(f32[2048]{0:T(1024)} %param.15) | copy-start | bytes 24580
  10.9 149.3 %all-gather.12.cloned.1.call-start = ((), (), s32[]{:S(2)}) async-start(), calls=%async_computation.7 | async-start | bytes 2621440 | tf_op jit(solution)/shard_map/all_gather | solution.py:99
  37.9 24.2 %all-to-all-start.1 = ((bf16[32,64,128]{2,1,0:T(8,128)(2,1)}), bf16[32,64,128]{2,1,0:T(8,128)(2,1)S(1)}, u32[]{:S(2)}, u32[]{:S(2)}) async-start(bf16[32,64,128]{2,1,0:T(8,128)(2,1)} %bitcast.13), calls=%async_computation.1 | async-start | bytes 1048576 | tf_op jit(solution)/shard_map/all_to_all | solution.py:117
  62.1 24.2 %all-to-all-start.2 = ((bf16[32,64,128]{2,1,0:T(8,128)(2,1)}), bf16[32,64,128]{2,1,0:T(8,128)(2,1)S(1)}, u32[]{:S(2)}, u32[]{:S(2)}) async-start(bf16[32,64,128]{2,1,0:T(8,128)(2,1)} %bitcast.138), calls=%async_computation.2 | async-start | bytes 1048576 | tf_op jit(solution)/shard_map/all_to_all | solution.py:103
  82.5 9.8 %copy-start.6 = (f32[4,512]{1,0:T(4,128)S(1)}, f32[4,512]{1,0:T(4,128)}, u32[]{:S(2)}) copy-start(f32[4,512]{1,0:T(4,128)} %param.21) | copy-start | bytes 24580
  82.5 9.9 %copy-start.9 = (f32[512]{0:T(512)S(1)}, f32[512]{0:T(512)}, u32[]{:S(2)}) copy-start(f32[512]{0:T(512)} %param.20) | copy-start | bytes 6148
  86.3 20.5 %all-to-all-start = ((bf16[32,64,128]{2,1,0:T(8,128)(2,1)}), bf16[32,64,128]{2,1,0:T(8,128)(2,1)}, u32[]{:S(2)}, u32[]{:S(2)}) async-start(bf16[32,64,128]{2,1,0:T(8,128)(2,1)} %bitcast.137), calls=%async_computation | async-start | bytes 1048576 | tf_op jit(solution)/shard_map/all_to_all | solution.py:110
  91.8 83.1 %all-gather.14.cloned.1.call-start = ((), (), s32[]{:S(2)}) async-start(), calls=%async_computation.8 | async-start | bytes 2621440 | tf_op jit(solution)/shard_map/all_gather | solution.py:147
  93.1 16.8 %copy-start = (f32[4,128,128]{2,1,0:T(8,128)S(1)}, f32[4,128,128]{2,1,0:T(8,128)}, u32[]{:S(2)}) copy-start(f32[4,128,128]{2,1,0:T(8,128)} %param.22) | copy-start | bytes 786436
  109.8 43.7 %copy-start.7 = (f32[128]{0:T(128)S(1)}, f32[128]{0:T(128)}, u32[]{:S(2)}) copy-start(f32[128]{0:T(128)} %param.23) | copy-start | bytes 1540
  153.4 6.7 %copy-start.2 = (bf16[8,64,2048]{2,1,0:T(8,128)(2,1)S(1)}, bf16[8,64,2048]{2,1,0:T(8,128)(2,1)}, u32[]{:S(2)}) copy-start(bf16[8,64,2048]{2,1,0:T(8,128)(2,1)} %param.14) | copy-start | bytes 6291460
  156.4 18.3 %all-to-all-start.3 = ((bf16[4,512,128]{2,0,1:T(4,128)(2,1)}), bf16[4,512,128]{2,0,1:T(4,128)(2,1)S(1)}, u32[]{:S(2)}, u32[]{:S(2)}) async-start(bf16[4,512,128]{2,0,1:T(4,128)(2,1)} %copy.34), calls=%async_computation.3 | async-start | bytes 1048576 | tf_op jit(solution)/shard_map/all_to_all | solution.py:137
  174.9 3.0 %copy-start.5 = (f32[2048]{0:T(1024)S(1)}, f32[2048]{0:T(1024)}, u32[]{:S(2)}) copy-start(f32[2048]{0:T(1024)} %param.25) | copy-start | bytes 24580
Sparse Core Ops, SparseCore 0:
  8.9 25.2 all-gather.7
  35.8 22.5 all-gather.9
  59.9 22.5 all-gather.5
  84.0 22.5 all-gather.11
  108.0 22.5 all-gather.13
where the time goes:
time: 187 us; the launch traced here: 186 us
  waiting for transfers between devices  75.9 us (41%)
  matrix products  50.2 us (27%)
  starting transfers between devices  20.4 us (11%)
  local copies, waits for them, and re-layouts  15.9 us (9%)
  between operations  13.3 us (7%)
  other arithmetic  10.2 us (5%)
    all_gather x1, waiting for transfers between devices, body(): v_sum = project(columns, lax.all_gather(w_value, 'dp', axis=0, tiled=True))  20.6 us
    all_gather x1, waiting for transfers between devices, body(): f_sum = project(columns, lax.all_gather(w_forget, 'dp', axis=0, tiled=True))  15 us
    all_gather x1, waiting for transfers between devices, body(): q_sum = project(columns, lax.all_gather(w_query, 'dp', axis=0, tiled=True))  14.9 us
    dot_general x4, matrix products, project(): jnp.einsum('jbq,qom->jobm', norm_result, reshaped_input, preferred_elemen...  14 us
    all_to_all x1, waiting for transfers between devices, body(): lax.all_to_all(f_sum.astype(jnp.bfloat16).reshape(item_shape), 'sp', spli...  13.7 us
    dot_general x8, matrix products, block_step(): jnp.dot((key_block * jnp.exp(block_end[None, :] - cumulative)).T, value_b...  12.6 us
    all_to_all x1, waiting for transfers between devices, body(): lax.all_to_all(head_normed, 'sp', split_axis=1, concat_axis=0, tiled=True)  11 us
    dot_general x8, matrix products, block_step(): jnp.dot(query_scaled, key_scaled.T, precision=lax.Precision.HIGHEST)  10.1 us
  transfers between devices with their start and end apart: 9, of which 5 were waited for; matrix products, arithmetic and copies ran while one was open for 37% of the time, Pallas kernels for 0%

commit v1 on v0

v1 whole, which is shorter than its diff:
```python
import functools

import jax
import jax.numpy as jnp
from jax import lax
from jax.experimental import pallas as pl
from jax.experimental.pallas import tpu as pltpu
from jax.sharding import PartitionSpec as P

EPS = 1e-06
MESH = pl.DeviceIdType.MESH


def rms_scale(matrix, gain):
    widened = matrix.astype(jnp.float32)
    return widened * lax.rsqrt(jnp.mean(widened * widened, axis=-1, keepdims=True) + EPS) * gain


def gather_rows(pieces):
    ways = lax.axis_size("sp")
    share = pieces.shape[0] // ways
    mine = lax.dynamic_slice_in_dim(pieces, lax.axis_index("sp") * share, share, axis=0)
    return lax.all_gather(mine, ("dp", "sp"), axis=0, tiled=True)


def chain_kernel(
    n,
    heads,
    f_v_ref,
    q_g_ref,
    extra_ref,
    gap_ref,
    init_ref,
    gain_ref,
    out_ref,
    rbuf,
    sbuf,
    send_sem,
    recv_sem,
    init_sem,
):
    me = lax.axis_index("sp")
    items, hv, hk = rbuf.shape
    own = init_ref.shape[0]
    length = extra_ref.shape[1]
    seqs = items // heads
    cols = heads * hk

    barrier = pltpu.get_barrier_semaphore()
    for offset in range(1, n):
        pl.semaphore_signal(
            barrier, inc=1, device_id={"sp": lax.rem(me + offset, n)}, device_id_type=MESH
        )
    pl.semaphore_wait(barrier, n - 1)

    def init_copy(j):
        return pltpu.make_async_remote_copy(
            src_ref=init_ref.at[j],
            dst_ref=rbuf.at[me * own + j],
            send_sem=init_sem.at[j],
            recv_sem=recv_sem.at[me * own + j],
            device_id={"sp": 0},
            device_id_type=MESH,
        )

    def chain_copy(it):
        return pltpu.make_async_remote_copy(
            src_ref=sbuf.at[it],
            dst_ref=rbuf.at[it],
            send_sem=send_sem.at[it],
            recv_sem=recv_sem.at[it],
            device_id={"sp": lax.rem(me + 1, n)},
            device_id_type=MESH,
        )

    @pl.when(me > 0)
    def _():
        for j in range(own):
            init_copy(j).start()

    @pl.when(me == 0)
    def _():
        rbuf[0:own] = init_ref[...]

    row = lax.broadcasted_iota(jnp.int32, (length, length), 0)
    col = lax.broadcasted_iota(jnp.int32, (length, length), 1)
    causal = row >= col
    ones = causal.astype(jnp.float32)
    nt = (((1,), (1,)), ((), ()))
    tn = (((0,), (0,)), ((), ()))

    def sequence(s, carry):
        rows = pl.ds(pl.multiple_of(s * length, length), length)
        f_pre = f_v_ref[rows, 0:cols].astype(jnp.float32)
        keys = gap_ref[...] * jax.nn.sigmoid(-f_pre)
        extra = extra_ref[s]
        spread = jnp.concatenate(
            [jnp.broadcast_to(extra[:, h : h + 1], (length, hk)) for h in range(heads)], axis=1
        )
        decay = jnp.log1p(-keys) + spread
        cum = jnp.dot(
            ones, decay, precision=lax.Precision.HIGHEST, preferred_element_type=jnp.float32
        )
        end = cum[length - 1 : length, :]
        mid = cum[length // 2 : length // 2 + 1, :]
        keys_end = (keys * jnp.exp(end - cum)).astype(jnp.bfloat16)
        keys_mid = (keys * jnp.exp(mid - cum)).astype(jnp.bfloat16)
        end_decay = jnp.exp(end)
        q_pre = q_g_ref[rows, 0:cols].astype(jnp.float32)
        queries = q_pre * jax.nn.sigmoid(q_pre)
        q_carry = (queries * jnp.exp(cum)).astype(jnp.bfloat16)
        q_mid = (queries * jnp.exp(cum - mid)).astype(jnp.bfloat16)
        within = []
        added = []
        for h in range(heads):
            lanes = slice(h * hk, (h + 1) * hk)
            values = f_v_ref[rows, cols + h * hv : cols + (h + 1) * hv]
            added.append(
                lax.dot_general(
                    values, keys_end[:, lanes], tn, preferred_element_type=jnp.float32
                )
            )
            scores = lax.dot_general(
                q_mid[:, lanes], keys_mid[:, lanes], nt, preferred_element_type=jnp.float32
            )
            scores = jnp.where(causal, scores, 0.0).astype(jnp.bfloat16)
            within.append(jnp.dot(scores, values, preferred_element_type=jnp.float32))
        for h in range(heads):
            lanes = slice(h * hk, (h + 1) * hk)
            it = s * heads + h

            @pl.when(jnp.logical_or(me > 0, it >= own))
            def _():
                chain_copy(it).wait_recv()

            @pl.when(me < n - 1)
            def _():
                state = rbuf[it].astype(jnp.float32)
                sbuf[it] = (state * end_decay[:, lanes] + added[h]).astype(jnp.bfloat16)
                chain_copy(it).start()

        for h in range(heads):
            lanes = slice(h * hk, (h + 1) * hk)
            it = s * heads + h
            outs = within[h] + lax.dot_general(
                q_carry[:, lanes], rbuf[it], nt, preferred_element_type=jnp.float32
            )
            normed = rms_scale(outs, gain_ref[...]).astype(jnp.bfloat16).astype(jnp.float32)
            g_pre = q_g_ref[rows, cols + h * hv : cols + (h + 1) * hv].astype(jnp.float32)
            out_ref[rows, h * hv : (h + 1) * hv] = (
                normed * (g_pre * jax.nn.sigmoid(g_pre))
            ).astype(jnp.bfloat16)
        return carry

    lax.fori_loop(0, seqs, sequence, 0)

    @pl.when(me > 0)
    def _():
        for j in range(own):
            init_copy(j).wait_send()

    @pl.when(me < n - 1)
    def _():
        def done(it, carry):
            chain_copy(it).wait_send()
            return carry

        lax.fori_loop(0, items, done, 0)


def recurrence(f_v, q_g, extra, gap, init, gain, heads, n):
    own, hv, hk = init.shape
    items = own * n
    vmem = pl.BlockSpec(memory_space=pltpu.VMEM)
    return pl.pallas_call(
        functools.partial(chain_kernel, n, heads),
        out_shape=jax.ShapeDtypeStruct((f_v.shape[0], heads * hv), jnp.bfloat16),
        in_specs=[vmem] * 6,
        out_specs=vmem,
        scratch_shapes=[
            pltpu.VMEM((items, hv, hk), jnp.bfloat16),
            pltpu.VMEM((items, hv, hk), jnp.bfloat16),
            pltpu.SemaphoreType.DMA((items,)),
            pltpu.SemaphoreType.DMA((items,)),
            pltpu.SemaphoreType.DMA((own,)),
        ],
        compiler_params=pltpu.CompilerParams(
            collective_id=0, has_side_effects=True, vmem_limit_bytes=24 * 1024 * 1024
        ),
        cost_estimate=pl.CostEstimate(flops=10**9, bytes_accessed=10**8, transcendentals=10**6),
    )(f_v, q_g, extra, gap, init, gain)


def body(
    n,
    tokens,
    pre_gain,
    w_query,
    w_forget,
    w_value,
    w_gate,
    lower_bound,
    extra_decay,
    initial_state,
    norm_gain,
    w_out,
    post_gain,
):
    seq_count, local_len, width = tokens.shape
    own, hk, hv = initial_state.shape
    heads = w_query.shape[1] // hk
    w_f_v = gather_rows(jnp.concatenate([w_forget, w_value], axis=1))
    w_q_g = gather_rows(jnp.concatenate([w_query, w_gate], axis=1))
    w_o = gather_rows(w_out)
    extra = lax.all_to_all(extra_decay, "sp", split_axis=1, concat_axis=0, tiled=True)
    extra = extra.reshape(seq_count, heads, local_len).transpose(0, 2, 1)
    init = jnp.swapaxes(initial_state, 1, 2).astype(jnp.bfloat16)
    normed = rms_scale(tokens, pre_gain).astype(jnp.bfloat16).reshape(seq_count * local_len, width)
    f_v = jnp.dot(normed, w_f_v, preferred_element_type=jnp.float32).astype(jnp.bfloat16)
    q_g = jnp.dot(normed, w_q_g, preferred_element_type=jnp.float32).astype(jnp.bfloat16)
    gated = recurrence(
        f_v, q_g, extra, (1.0 - lower_bound)[None, :], init, norm_gain[None, :], heads, n
    )
    mixed = jnp.dot(gated, w_o, preferred_element_type=jnp.float32)
    return rms_scale(mixed, post_gain).astype(jnp.bfloat16).reshape(seq_count, local_len, width)


def solution(mesh):
    in_specs = (
        P("dp", "sp", None),
        P(),
        P("dp", None),
        P("dp", None),
        P("dp", None),
        P("dp", None),
        P(),
        P(("dp", "sp"), None),
        P(("dp", "sp"), None, None),
        P(),
        P("dp", None),
        P(),
    )
    out_specs = P("dp", "sp", None)
    return jax.shard_map(
        functools.partial(body, mesh.shape["sp"]),
        mesh=mesh,
        in_specs=in_specs,
        out_specs=out_specs,
        check_vma=False,
    )
```

time: 187 us -> 216 us (1.16)
  the two profiles are of different devices: /device:TPU:0 before, /device:TPU:26 now
where the time goes in v1:
time: 216 us
  waiting for transfers between devices  108 us (50%)
  Pallas kernels  64.7 us (30%)
  matrix products  13.2 us (6%)
  between operations  13.2 us (6%)
  other arithmetic  7.96 us (4%)
  starting transfers between devices  6.08 us (3%)
  local copies, waits for them, and re-layouts  2.99 us (1%)
    all_gather x3, waiting for transfers between devices, gather_rows(): return lax.all_gather(mine, ('dp', 'sp'), axis=0, tiled=True)  108 us
    pallas_call x1, Pallas kernels, recurrence(): pl.pallas_call(functools.partial(chain_kernel, n, heads), out_shape=jax.S...  64.7 us
    all_to_all x1, starting transfers between devices, body(): lax.all_to_all(extra_decay, 'sp', split_axis=1, concat_axis=0, tiled=True)  6 us
    dot_general x1, matrix products, body(): jnp.dot(normed, w_f_v, preferred_element_type=jnp.float32)  5.15 us
    dot_general x1, matrix products, body(): jnp.dot(normed, w_q_g, preferred_element_type=jnp.float32)  5.15 us
  transfers between devices with their start and end apart: 4, of which 2 were waited for; matrix products, arithmetic and copies ran while one was open for 8% of the time, Pallas kernels for 30%

profile of v1, /device:TPU:26, one launch (start us, length us, event | category | flops | bytes accessed | tf_op | source)
XLA Modules:
  0.0 216.1 jit_solution(3225185645645666659)
XLA Ops:
  6.5 0.0 copy-start
  6.5 0.0 copy-start.2
  6.5 0.0 copy-start.4
  6.5 0.0 all-gather.6.cloned.1.call-start
  6.6 1.7 fusion.3
  8.2 0.0 copy-start.6
  8.2 0.0 copy-start.3
  8.2 0.0 all-gather.6.cloned.1.call-update
  8.3 0.0 all-gather.4.cloned.1.call-start
  8.3 1.6 fusion.4
  9.9 0.0 all-gather.4.cloned.1.call-update
  9.9 0.0 all-gather.8.cloned.1.call-start
  10.0 0.0 copy-done
  10.0 0.6 constant_dynamic-slice_fusion
  10.6 0.0 all-gather.8.cloned.1.call-update
  10.7 0.8 all_to_all.10
  11.5 0.7 reshape.31
  12.1 6.0 %all-to-all-start = ((f32[8,1,256]{2,1,0:T(1,128)}), f32[8,1,256]{2,1,0:T(1,128)S(1)}, u32[]{:S(2)}, u32[]{:S(2)}) async-start(f32[8,1,256]{2,1,0:T(1,128)} %reshape.31), calls=%async_computation | async-start | bytes 16384 | tf_op jit(solution)/shard_map/all_to_all | solution.py:215
  18.1 0.0 copy-done.2
  18.1 0.5 fusion
  18.6 0.0 copy-done.4
  18.6 1.9 fusion.2
  20.5 0.0 copy-done.6
  20.5 0.0 copy-done.3
  20.5 0.1 copy.19
  20.6 0.0 all-to-all-done
  20.6 0.5 broadcast.24
  21.1 0.6 reduce
  21.7 0.1 reshape.32
  21.8 0.2 copy.18
  22.0 49.6 %all-gather.6.cloned.1.call-done = bf16[2048,1024]{1,0:T(8,128)(2,1)} async-done(((bf16[64,1024]{1,0:T(8,128)(2,1)}), bf16[2048,1024]{1,0:T(8,128)(2,1)}) %all-gather.6.cloned.1.call-update) | async-done | bytes 4194320 | tf_op jit(solution)/shard_map/all_gather | solution.py:23
  71.5 5.1 %convolution_convert_fusion.q_g_ref = bf16[512,1024]{1,0:T(8,128)(2,1)S(1)} fusion(bf16[512,2048]{1,0:T(8,128)(2,1)} %bitcast.22, bf16[2048,1024]{1,0:T(8,128)(2,1)} %all-gather.6.cloned.1.call-done), kind=kOutput, calls=%fused_computation.7 | convolution fusion | flops 2148007936 | bytes 7340032 | tf_op jit(solution)/shard_map/dot_general | solution.py:220
  76.7 0.0 copy-start.1
  76.7 58.3 %all-gather.4.cloned.1.call-done = bf16[2048,1024]{1,0:T(8,128)(2,1)} async-done(((bf16[64,1024]{1,0:T(8,128)(2,1)}), bf16[2048,1024]{1,0:T(8,128)(2,1)}) %all-gather.4.cloned.1.call-update) | async-done | bytes 4194320 | tf_op jit(solution)/shard_map/all_gather | solution.py:23
  135.0 5.2 %convolution_convert_fusion.1.f_v_ref = bf16[512,1024]{1,0:T(8,128)(2,1)S(1)} fusion(bf16[512,2048]{1,0:T(8,128)(2,1)} %bitcast.23, bf16[2048,1024]{1,0:T(8,128)(2,1)} %all-gather.4.cloned.1.call-done), kind=kOutput, calls=%fused_computation.8 | convolution fusion | flops 2148007936 | bytes 7340032 | tf_op jit(solution)/shard_map/dot_general | solution.py:219
  140.1 0.0 copy-done.1
  140.2 64.7 %shard_map.118 = bf16[512,512]{1,0:T(8,128)(2,1)S(1)} custom-call(bf16[512,1024]{1,0:T(8,128)(2,1)S(1)} %convolution_convert_fusion.1.f_v_ref, bf16[512,1024]{1,0:T(8,128)(2,1)S(1)} %convolution_convert_fusion.q_g_ref, f32[8,64,4]{2,1,0:T(8,128)S(1)} %bitcast.18, f32[1,512]{1,0:T(1,128)S(1)} %bitcast.20, bf16[4,128,128]{2,1,0:T(8,128)(2,1)S(1)} %bitcast.19, ...), custom_call_target="tpu_custom_call" | custom-call | flops 1000000000 | bytes 100000000 | tf_op jit(solution)/shard_map/pallas_call | solution.py:175
  204.9 0.0 copy-start.5
  204.9 0.0 all-gather.8.cloned.1.call-done
  204.9 2.9 %multiply_reduce_fusion = (f32[512]{0:T(512)S(1)}, f32[512,2048]{1,0:T(8,128)S(1)}) fusion(bf16[512,512]{1,0:T(8,128)(2,1)S(1)} %shard_map.118, bf16[512,2048]{1,0:T(8,128)(2,1)} %all-gather.8.cloned.1.call-done), kind=kOutput, calls=%fused_computation.6 | convolution fusion | flops 1075838464 | bytes 6817792 | tf_op jit(solution)/shard_map/dot_general | solution.py:224
  207.8 0.0 copy-done.5
  207.9 1.7 multiply_convert_fusion
  (4 shorter events, 0.0 us)
Async XLA Ops:
  6.5 3.4 %copy-start = (bf16[128,2048]{1,0:T(8,128)(2,1)S(1)}, bf16[128,2048]{1,0:T(8,128)(2,1)}, u32[]{:S(2)}) copy-start(bf16[128,2048]{1,0:T(8,128)(2,1)} %param.22) | copy-start | bytes 1572868
  6.5 11.6 %copy-start.2 = (bf16[8,64,2048]{2,1,0:T(8,128)(2,1)S(1)}, bf16[8,64,2048]{2,1,0:T(8,128)(2,1)}, u32[]{:S(2)}) copy-start(bf16[8,64,2048]{2,1,0:T(8,128)(2,1)} %param.12) | copy-start | bytes 6291460
  6.5 12.1 %copy-start.4 = (f32[2048]{0:T(1024)S(1)}, f32[2048]{0:T(1024)}, u32[]{:S(2)}) copy-start(f32[2048]{0:T(1024)} %param.13) | copy-start | bytes 24580
  6.5 65.0 %all-gather.6.cloned.1.call-start = ((), (), s32[]{:S(2)}) async-start(), calls=%async_computation.2 | async-start | bytes 4325376 | tf_op jit(solution)/shard_map/all_gather | solution.py:23
  8.2 12.3 %copy-start.6 = (f32[512]{0:T(512)S(1)}, f32[512]{0:T(512)}, u32[]{:S(2)}) copy-start(f32[512]{0:T(512)} %param.18) | copy-start | bytes 6148
  8.2 12.3 %copy-start.3 = (f32[4,128,128]{2,1,0:T(8,128)S(1)}, f32[4,128,128]{2,1,0:T(8,128)}, u32[]{:S(2)}) copy-start(f32[4,128,128]{2,1,0:T(8,128)} %param.20) | copy-start | bytes 786436
  8.3 126.7 %all-gather.4.cloned.1.call-start = ((), (), s32[]{:S(2)}) async-start(), calls=%async_computation.1 | async-start | bytes 4325376 | tf_op jit(solution)/shard_map/all_gather | solution.py:23
  9.9 195.0 %all-gather.8.cloned.1.call-start = ((), (), s32[]{:S(2)}) async-start(), calls=%async_computation.3 | async-start | bytes 2162688 | tf_op jit(solution)/shard_map/all_gather | solution.py:23
  12.1 8.5 %all-to-all-start = ((f32[8,1,256]{2,1,0:T(1,128)}), f32[8,1,256]{2,1,0:T(1,128)S(1)}, u32[]{:S(2)}, u32[]{:S(2)}) async-start(f32[8,1,256]{2,1,0:T(1,128)} %reshape.31), calls=%async_computation | async-start | bytes 16384 | tf_op jit(solution)/shard_map/all_to_all | solution.py:215
  76.7 63.5 %copy-start.1 = (f32[128]{0:T(128)S(1)}, f32[128]{0:T(128)}, u32[]{:S(2)}) copy-start(f32[128]{0:T(128)} %param.21) | copy-start | bytes 1540
  204.9 3.0 %copy-start.5 = (f32[2048]{0:T(1024)S(1)}, f32[2048]{0:T(1024)}, u32[]{:S(2)}) copy-start(f32[2048]{0:T(1024)} %param.23) | copy-start | bytes 24580
Sparse Core Ops, SparseCore 0:
  10.3 61.1 all-gather.5
  74.5 60.4 all-gather.3
  138.0 61.8 all-gather.7

commit v2 on v1

v2 whole, which is shorter than its diff:
```python
import functools

import jax
import jax.numpy as jnp
from jax import lax
from jax.experimental import pallas as pl
from jax.experimental.pallas import tpu as pltpu
from jax.sharding import PartitionSpec as P

EPS = 1e-06
MESH = pl.DeviceIdType.MESH


def rms_scale(matrix, gain):
    widened = matrix.astype(jnp.float32)
    return widened * lax.rsqrt(jnp.mean(widened * widened, axis=-1, keepdims=True) + EPS) * gain


def layer_kernel(
    n,
    ways,
    heads,
    tokens_ref,
    pre_ref,
    w0,
    w1,
    w2,
    w3,
    w4,
    extra_ref,
    gap_ref,
    init_ref,
    gain_ref,
    out_ref,
    a4,
    a0,
    a1,
    a2,
    a3,
    normed,
    f_v_ref,
    q_g_ref,
    cum_ref,
    keys_ref,
    rbuf,
    sbuf,
    send_sem,
    recv_sem,
    init_sem,
    y_send,
    y_recv,
    x_send,
    x_recv,
    s_send,
    s_recv,
    local_sem,
):
    me = lax.axis_index("sp")
    rank = lax.axis_index("dp")
    items, hv, hk = rbuf.shape
    own = init_ref.shape[0]
    seqs, length, width = tokens_ref.shape
    cols = heads * hk
    tile = 2 * hk
    shards = (w0, w1, w2, w3, w4)
    wholes = (a0, a1, a2, a3, a4)
    side = lax.rem(me, 2)
    beside = me + 1 - 2 * side
    sibling = rank + 1 - 2 * lax.rem(rank, 2)
    peers = ways // 2 - 1

    barrier = pltpu.get_barrier_semaphore()
    for offset in range(1, n):
        pl.semaphore_signal(
            barrier, inc=1, device_id={"sp": lax.rem(me + offset, n)}, device_id_type=MESH
        )
    for offset in range(1, ways):
        pl.semaphore_signal(
            barrier, inc=1, device_id={"dp": lax.rem(rank + offset, ways)}, device_id_type=MESH
        )
    pl.semaphore_wait(barrier, n + ways - 2)

    def part(w, shard, half):
        rows = shards[w].shape[0]
        start = shard * rows + half * (rows // 2)
        return wholes[w].at[pl.ds(pl.multiple_of(start, rows // 2), rows // 2)]

    def full(w, shard):
        rows = shards[w].shape[0]
        return wholes[w].at[pl.ds(pl.multiple_of(shard * rows, rows), rows)]

    def remote(src, dst, send, recv, device):
        return pltpu.make_async_remote_copy(
            src_ref=src,
            dst_ref=dst,
            send_sem=send,
            recv_sem=recv,
            device_id=device,
            device_id_type=MESH,
        )

    def y_copy(w, k):
        rows = shards[w].shape[0] // 2
        src = shards[w].at[pl.ds(pl.multiple_of(side * rows, rows), rows)]
        target = lax.rem(rank + 2 * (k + 1), ways)
        return remote(src, part(w, rank, side), y_send.at[w, k], y_recv.at[w, k], {"dp": target})

    def origin(k):
        return lax.rem(rank + ways - 2 * (k + 1), ways)

    def x_copy(w, k):
        ref = part(w, origin(k), side)
        return remote(ref, ref, x_send.at[w, k], x_recv.at[w, k], {"sp": beside})

    def s_own(w):
        return remote(
            shards[w], full(w, rank), s_send.at[w, 0], s_recv.at[w, 0], {"dp": sibling}
        )

    def s_copy(w, k, second):
        ref = part(w, origin(k), 1 - side if second else side)
        slot = 1 + 2 * k + second
        return remote(ref, ref, s_send.at[w, slot], s_recv.at[w, slot], {"dp": sibling})

    def local_copy(w):
        return pltpu.make_async_copy(shards[w], full(w, rank), local_sem.at[w])

    def pass_y(w):
        for k in range(peers):
            y_copy(w, k).wait_recv()
            x_copy(w, k).start()
            s_copy(w, k, 0).start()

    def pass_x(w):
        for k in range(peers):
            x_copy(w, k).wait_recv()
            s_copy(w, k, 1).start()

    def arrived(w):
        s_own(w).wait_recv()
        for k in range(peers):
            s_copy(w, k, 0).wait_recv()
            s_copy(w, k, 1).wait_recv()

    def init_copy(j):
        return remote(
            init_ref.at[j],
            rbuf.at[me * own + j],
            init_sem.at[j],
            recv_sem.at[me * own + j],
            {"sp": 0},
        )

    def chain_copy(it):
        return remote(
            sbuf.at[it],
            rbuf.at[it],
            send_sem.at[it],
            recv_sem.at[it],
            {"sp": lax.rem(me + 1, n)},
        )

    for w in range(5):
        for k in range(peers):
            y_copy(w, k).start()
        s_own(w).start()
        local_copy(w).start()

    @pl.when(me > 0)
    def _():
        for j in range(own):
            init_copy(j).start()

    @pl.when(me == 0)
    def _():
        rbuf[0:own] = init_ref[...]

    def norm_rows(s, carry):
        rows = pl.ds(pl.multiple_of(s * length, length), length)
        normed[rows, :] = rms_scale(tokens_ref[s], pre_ref[...]).astype(jnp.bfloat16)
        return carry

    lax.fori_loop(0, seqs, norm_rows, 0)

    def project(w, dest, at, j):
        lanes = pl.ds(pl.multiple_of(j * tile, tile), tile)
        where = pl.ds(pl.multiple_of(at + j * tile, tile), tile)
        dest[:, where] = jnp.dot(
            normed[...], wholes[w][:, lanes], preferred_element_type=jnp.float32
        ).astype(jnp.bfloat16)

    def project_all(w, dest, at):
        def step(j, carry):
            project(w, dest, at, j)
            return carry

        lax.fori_loop(0, cols // tile, step, 0)

    for w in range(5):
        local_copy(w).wait()
    pass_y(0)
    pass_y(1)
    pass_x(0)
    arrived(0)
    project_all(0, f_v_ref, 0)
    pass_x(1)
    pass_y(2)
    arrived(1)
    project_all(1, f_v_ref, cols)
    pass_x(2)
    pass_y(3)
    pass_x(3)
    pass_y(4)

    row = lax.broadcasted_iota(jnp.int32, (length, length), 0)
    col = lax.broadcasted_iota(jnp.int32, (length, length), 1)
    causal = row >= col
    ones = causal.astype(jnp.float32)
    nt = (((1,), (1,)), ((), ()))
    tn = (((0,), (0,)), ((), ()))
    tiles = cols // tile

    def forward(s, carry):
        rows = pl.ds(pl.multiple_of(s * length, length), length)
        f_pre = f_v_ref[rows, 0:cols].astype(jnp.float32)
        keys = gap_ref[...] * jax.nn.sigmoid(-f_pre)
        extra = extra_ref[s]
        spread = jnp.concatenate(
            [jnp.broadcast_to(extra[:, h : h + 1], (length, hk)) for h in range(heads)], axis=1
        )
        decay = jnp.log1p(-keys) + spread
        cum = jnp.dot(
            ones, decay, precision=lax.Precision.HIGHEST, preferred_element_type=jnp.float32
        )
        end = cum[length - 1 : length, :]
        mid = cum[length // 2 : length // 2 + 1, :]
        keys_end = (keys * jnp.exp(end - cum)).astype(jnp.bfloat16)
        keys_ref[rows, :] = (keys * jnp.exp(mid - cum)).astype(jnp.bfloat16)
        cum_ref[rows, :] = cum
        end_decay = jnp.exp(end)
        added = []
        for h in range(heads):
            lanes = slice(h * hk, (h + 1) * hk)
            values = f_v_ref[rows, cols + h * hv : cols + (h + 1) * hv]
            added.append(
                lax.dot_general(
                    values, keys_end[:, lanes], tn, preferred_element_type=jnp.float32
                )
            )
        for h in range(heads):
            lanes = slice(h * hk, (h + 1) * hk)
            it = s * heads + h

            @pl.when(jnp.logical_or(me > 0, it >= own))
            def _():
                chain_copy(it).wait_recv()

            @pl.when(me < n - 1)
            def _():
                state = rbuf[it].astype(jnp.float32)
                sbuf[it] = (state * end_decay[:, lanes] + added[h]).astype(jnp.bfloat16)
                chain_copy(it).start()

        @pl.when(s == 0)
        def _():
            arrived(2)

        @pl.when(s == tiles)
        def _():
            arrived(3)

        @pl.when(s < tiles)
        def _():
            project(2, q_g_ref, 0, s)

        @pl.when(jnp.logical_and(s >= tiles, s < 2 * tiles))
        def _():
            project(3, q_g_ref, cols, s - tiles)

        return carry

    lax.fori_loop(0, seqs, forward, 0)
    pass_x(4)

    def outputs(s, carry):
        rows = pl.ds(pl.multiple_of(s * length, length), length)
        cum = cum_ref[rows, :]
        mid = cum[length // 2 : length // 2 + 1, :]
        q_pre = q_g_ref[rows, 0:cols].astype(jnp.float32)
        queries = q_pre * jax.nn.sigmoid(q_pre)
        q_carry = (queries * jnp.exp(cum)).astype(jnp.bfloat16)
        q_mid = (queries * jnp.exp(cum - mid)).astype(jnp.bfloat16)
        for h in range(heads):
            lanes = slice(h * hk, (h + 1) * hk)
            it = s * heads + h
            values = f_v_ref[rows, cols + h * hv : cols + (h + 1) * hv]
            scores = lax.dot_general(
                q_mid[:, lanes], keys_ref[rows, lanes], nt, preferred_element_type=jnp.float32
            )
            scores = jnp.where(causal, scores, 0.0).astype(jnp.bfloat16)
            outs = jnp.dot(scores, values, preferred_element_type=jnp.float32) + lax.dot_general(
                q_carry[:, lanes], rbuf[it], nt, preferred_element_type=jnp.float32
            )
            scaled = rms_scale(outs, gain_ref[...]).astype(jnp.bfloat16).astype(jnp.float32)
            g_pre = q_g_ref[rows, cols + h * hv : cols + (h + 1) * hv].astype(jnp.float32)
            out_ref[rows, h * hv : (h + 1) * hv] = (
                scaled * (g_pre * jax.nn.sigmoid(g_pre))
            ).astype(jnp.bfloat16)
        return carry

    lax.fori_loop(0, seqs, outputs, 0)
    arrived(4)
    for w in range(5):
        s_own(w).wait_send()
        for k in range(peers):
            y_copy(w, k).wait_send()
            x_copy(w, k).wait_send()
            s_copy(w, k, 0).wait_send()
            s_copy(w, k, 1).wait_send()

    @pl.when(me > 0)
    def _():
        for j in range(own):
            init_copy(j).wait_send()

    @pl.when(me < n - 1)
    def _():
        def done(it, carry):
            chain_copy(it).wait_send()
            return carry

        lax.fori_loop(0, items, done, 0)


def layer(tokens, pre, weights, extra, gap, init, gain, n, ways):
    own, hv, hk = init.shape
    seqs, length, width = tokens.shape
    items = own * n
    heads = items // seqs
    rows = seqs * length
    peers = max(ways // 2 - 1, 1)
    vmem = pl.BlockSpec(memory_space=pltpu.VMEM)
    dma = pltpu.SemaphoreType.DMA

    def whole(w):
        return (w.shape[0] * ways, w.shape[1])

    return pl.pallas_call(
        functools.partial(layer_kernel, n, ways, heads),
        out_shape=[
            jax.ShapeDtypeStruct((rows, heads * hv), jnp.bfloat16),
            jax.ShapeDtypeStruct(whole(weights[4]), jnp.bfloat16),
        ],
        in_specs=[vmem] * 11,
        out_specs=[vmem] * 2,
        scratch_shapes=[pltpu.VMEM(whole(w), jnp.bfloat16) for w in weights[:4]]
        + [
            pltpu.VMEM((rows, width), jnp.bfloat16),
            pltpu.VMEM((rows, heads * (hk + hv)), jnp.bfloat16),
            pltpu.VMEM((rows, heads * (hk + hv)), jnp.bfloat16),
            pltpu.VMEM((rows, heads * hk), jnp.float32),
            pltpu.VMEM((rows, heads * hk), jnp.bfloat16),
            pltpu.VMEM((items, hv, hk), jnp.bfloat16),
            pltpu.VMEM((items, hv, hk), jnp.bfloat16),
            dma((items,)),
            dma((items,)),
            dma((own,)),
            dma((5, peers)),
            dma((5, peers)),
            dma((5, peers)),
            dma((5, peers)),
            dma((5, 1 + 2 * peers)),
            dma((5, 1 + 2 * peers)),
            dma((5,)),
        ],
        compiler_params=pltpu.CompilerParams(
            collective_id=0, has_side_effects=True, vmem_limit_bytes=48 * 1024 * 1024
        ),
        cost_estimate=pl.CostEstimate(
            flops=6 * 10**9, bytes_accessed=2 * 10**7, transcendentals=10**6
        ),
    )(tokens, pre, *weights, extra, gap, init, gain)


def body(
    n,
    ways,
    tokens,
    pre_gain,
    w_query,
    w_forget,
    w_value,
    w_gate,
    lower_bound,
    extra_decay,
    initial_state,
    norm_gain,
    w_out,
    post_gain,
):
    seq_count, local_len, width = tokens.shape
    heads = w_query.shape[1] // initial_state.shape[1]
    extra = lax.all_to_all(extra_decay, "sp", split_axis=1, concat_axis=0, tiled=True)
    extra = extra.reshape(seq_count, heads, local_len).transpose(0, 2, 1)
    init = jnp.swapaxes(initial_state, 1, 2).astype(jnp.bfloat16)
    gated, w_o = layer(
        tokens,
        pre_gain[None, :],
        (w_forget, w_value, w_query, w_gate, w_out),
        extra,
        (1.0 - lower_bound)[None, :],
        init,
        norm_gain[None, :],
        n,
        ways,
    )
    mixed = jnp.dot(gated, w_o, preferred_element_type=jnp.float32)
    return rms_scale(mixed, post_gain).astype(jnp.bfloat16).reshape(seq_count, local_len, width)


def solution(mesh):
    in_specs = (
        P("dp", "sp", None),
        P(),
        P("dp", None),
        P("dp", None),
        P("dp", None),
        P("dp", None),
        P(),
        P(("dp", "sp"), None),
        P(("dp", "sp"), None, None),
        P(),
        P("dp", None),
        P(),
    )
    out_specs = P("dp", "sp", None)
    return jax.shard_map(
        functools.partial(body, mesh.shape["sp"], mesh.shape["dp"]),
        mesh=mesh,
        in_specs=in_specs,
        out_specs=out_specs,
        check_vma=False,
    )
```

time: 216 us -> 119 us (0.55)
  waiting for transfers between devices: 108 us -> 0.64 us
  Pallas kernels: 64.7 us -> 97.6 us
  between operations: 13.2 us -> 0.06 us
  matrix products: 13.2 us -> 1.35 us
  local copies, waits for them, and re-layouts: 2.99 us -> 9.84 us
  other arithmetic: 7.96 us -> 3.09 us
    all_gather x3 -> x0, waiting for transfers between devices: 108 us -> none  [gather_rows(): return lax.all_gather(mine, ('dp', 'sp'), axis=0, tiled=True)]
    pallas_call x1, Pallas kernels: 64.7 us -> 97.6 us  [layer(): pl.pallas_call(functools.partial(layer_kernel, n, ways, heads), out_shape...]
    dot_general x2 -> x0, matrix products: 10.3 us -> none  [the longest x1 5.15 us: body(): jnp.dot(normed, w_f_v, preferred_element_type=jnp.float32)]
    unnamed x17 -> x19, local copies, waits for them, and re-layouts: 0.91 us -> 8.39 us
    concatenate x2 -> x0, other arithmetic: 3.27 us -> none  [the longest x1 1.68 us: body(): w_q_g = gather_rows(jnp.concatenate([w_query, w_gate], axis=1))]
  transfers between devices with their start and end apart: 4 -> 1, of which waited for: 2 -> 1; matrix products, arithmetic and copies ran while one was open for 8% -> 1% of each run, Pallas kernels for 30% -> 0%
where the time goes in v2:
time: 119 us
  Pallas kernels  97.6 us (82%)
  local copies, waits for them, and re-layouts  9.84 us (8%)
  starting transfers between devices  6 us (5%)
  other arithmetic  3.09 us (3%)
  matrix products  1.35 us (1%)
    pallas_call x1, Pallas kernels, layer(): pl.pallas_call(functools.partial(layer_kernel, n, ways, heads), out_shape...  97.6 us
    unnamed x19, local copies, waits for them, and re-layouts  8.39 us
    all_to_all x1, starting transfers between devices, body(): lax.all_to_all(extra_decay, 'sp', split_axis=1, concat_axis=0, tiled=True)  6 us
  transfers between devices with their start and end apart: 1, of which 1 were waited for; matrix products, arithmetic and copies ran while one was open for 1% of the time, Pallas kernels for 0%

profile of v2, /device:TPU:26, one launch (start us, length us, event | category | flops | bytes accessed | tf_op | source)
XLA Modules:
  0.0 118.6 jit_solution(5585229780051084471)
XLA Ops:
  0.0 0.8 all_to_all.10
  0.8 0.7 reshape.18
  1.5 6.0 %all-to-all-start = ((f32[8,1,256]{2,1,0:T(1,128)}), f32[8,1,256]{2,1,0:T(1,128)S(1)}, u32[]{:S(2)}, u32[]{:S(2)}) async-start(f32[8,1,256]{2,1,0:T(1,128)} %reshape.18), calls=%async_computation | async-start | bytes 16384 | tf_op jit(solution)/shard_map/all_to_all | solution.py:403
  7.5 0.7 broadcast_subtract_fusion
  8.2 1.1 copy.19
  9.2 0.6 all-to-all-done
  9.9 0.5 broadcast.12
  10.4 0.7 reduce
  11.0 0.1 reshape.19
  11.1 0.2 copy.18
  11.3 0.0 copy-start
  11.3 1.0 copy-done
  12.3 0.0 copy-start.1
  12.3 1.0 copy-done.1
  13.4 0.0 copy-start.2
  13.4 1.0 copy-done.2
  14.4 0.0 copy-start.3
  14.4 1.0 copy-done.3
  15.5 0.0 copy-start.4
  15.5 1.0 copy-done.4
  16.5 0.0 copy-start.5
  16.5 0.7 copy-done.5
  17.2 0.0 copy-start.6
  17.2 0.7 copy-done.6
  17.9 97.6 %shard_map.118 = (bf16[512,512]{1,0:T(8,128)(2,1)S(1)}, bf16[512,2048]{1,0:T(8,128)(2,1)S(1)}) custom-call(bf16[8,64,2048]{2,1,0:T(8,128)(2,1)} %tokens_ref.1, f32[1,2048]{1,0:T(1,128)S(1)} %bitcast.17, bf16[512,512]{1,0:T(8,128)(2,1)S(1)} %copy-done, bf16[512,512]{1,0:T(8,128)(2,1)S(1)} %copy-done.1, bf16[512,512]{1,0:T(8,128)(2,1)S(1)} %copy-done.2, ...), custom_call_target="tpu_custom_call" | custom-call | flops 6000000000 | bytes 20000000 | tf_op jit(solution)/shard_map/pallas_call | solution.py:348
  115.5 0.0 copy-start.7
  115.5 1.3 %multiply_reduce_fusion = (f32[512]{0:T(512)S(1)}, f32[512,2048]{1,0:T(8,128)S(1)}) fusion(bf16[512,512]{1,0:T(8,128)(2,1)S(1)} %get-tuple-element.7, bf16[512,2048]{1,0:T(8,128)(2,1)S(1)} %get-tuple-element.8), kind=kOutput, calls=%fused_computation.1 | convolution fusion | flops 1075838464 | bytes 6817792 | tf_op jit(solution)/shard_map/dot_general | solution.py:417
  116.8 0.0 copy-done.7
  116.9 1.7 %multiply_convert_fusion = bf16[512,2048]{1,0:T(8,128)(2,1)} fusion(f32[512,2048]{1,0:T(8,128)S(1)} %get-tuple-element.10, f32[2048]{0:T(1024)S(1)} %copy-done.7, f32[512]{0:T(512)S(1)} %add_rsqrt_fusion), kind=kLoop, calls=%fused_computation | loop fusion | flops 3145728 | bytes 6301696 | tf_op jit(solution)/shard_map/convert_element_type | solution.py:418
  (2 shorter events, 0.0 us)
Async XLA Ops:
  1.5 8.4 %all-to-all-start = ((f32[8,1,256]{2,1,0:T(1,128)}), f32[8,1,256]{2,1,0:T(1,128)S(1)}, u32[]{:S(2)}, u32[]{:S(2)}) async-start(f32[8,1,256]{2,1,0:T(1,128)} %reshape.18), calls=%async_computation | async-start | bytes 16384 | tf_op jit(solution)/shard_map/all_to_all | solution.py:403
  11.3 1.0 copy-start
  12.3 1.0 copy-start.1
  13.4 1.0 copy-start.2
  14.4 1.0 copy-start.3
  15.5 1.0 copy-start.4
  16.5 0.7 copy-start.5
  17.2 0.7 copy-start.6
  115.5 1.4 %copy-start.7 = (f32[2048]{0:T(1024)S(1)}, f32[2048]{0:T(1024)}, u32[]{:S(2)}) copy-start(f32[2048]{0:T(1024)} %param.23) | copy-start | bytes 24580

commit v3 on v2

--- a/solution.py
+++ b/solution.py
@@ -20,23 +20,31 @@
     n,
     ways,
     heads,
-    tokens_ref,
-    pre_ref,
+    tokens_hbm,
+    pre_hbm,
     w0,
     w1,
     w2,
     w3,
     w4,
-    extra_ref,
-    gap_ref,
-    init_ref,
-    gain_ref,
+    extra_hbm,
+    bound_hbm,
+    init_hbm,
+    gain_hbm,
     out_ref,
     a4,
     a0,
     a1,
     a2,
     a3,
+    tokens_ref,
+    pre_ref,
+    raw_ref,
+    extra_ref,
+    bound_ref,
+    start_ref,
+    init_ref,
+    gain_ref,
     normed,
     f_v_ref,
     q_g_ref,
@@ -54,6 +62,8 @@
     s_send,
     s_recv,
     local_sem,
+    e_send,
+    e_recv,
 ):
     me = lax.axis_index("sp")
     rank = lax.axis_index("dp")
@@ -69,6 +79,31 @@
     sibling = rank + 1 - 2 * lax.rem(rank, 2)
     peers = ways // 2 - 1
 
+    def local_copy(w):
+        return pltpu.make_async_copy(shards[w], full(w, rank), local_sem.at[w])
+
+    def full(w, shard):
+        rows = shards[w].shape[0]
+        return wholes[w].at[pl.ds(pl.multiple_of(shard * rows, rows), rows)]
+
+    small = [
+        pltpu.make_async_copy(src, dst, local_sem.at[5 + j])
+        for j, (src, dst) in enumerate(
+            (
+                (tokens_hbm, tokens_ref),
+                (pre_hbm, pre_ref),
+                (extra_hbm, raw_ref.at[me]),
+                (bound_hbm, bound_ref),
+                (init_hbm, start_ref),
+                (gain_hbm, gain_ref),
+            )
+        )
+    ]
+    for w in range(5):
+        local_copy(w).start()
+    for copy in small:
+        copy.start()
+
     barrier = pltpu.get_barrier_semaphore()
     for offset in range(1, n):
         pl.semaphore_signal(
@@ -84,10 +119,6 @@
         rows = shards[w].shape[0]
         start = shard * rows + half * (rows // 2)
         return wholes[w].at[pl.ds(pl.multiple_of(start, rows // 2), rows // 2)]
-
-    def full(w, shard):
-        rows = shards[w].shape[0]
-        return wholes[w].at[pl.ds(pl.multiple_of(shard * rows, rows), rows)]
 
     def remote(src, dst, send, recv, device):
         return pltpu.make_async_remote_copy(
@@ -100,10 +131,9 @@
         )
 
     def y_copy(w, k):
-        rows = shards[w].shape[0] // 2
-        src = shards[w].at[pl.ds(pl.multiple_of(side * rows, rows), rows)]
+        ref = part(w, rank, side)
         target = lax.rem(rank + 2 * (k + 1), ways)
-        return remote(src, part(w, rank, side), y_send.at[w, k], y_recv.at[w, k], {"dp": target})
+        return remote(ref, ref, y_send.at[w, k], y_recv.at[w, k], {"dp": target})
 
     def origin(k):
         return lax.rem(rank + ways - 2 * (k + 1), ways)
@@ -113,17 +143,13 @@
         return remote(ref, ref, x_send.at[w, k], x_recv.at[w, k], {"sp": beside})
 
     def s_own(w):
-        return remote(
-            shards[w], full(w, rank), s_send.at[w, 0], s_recv.at[w, 0], {"dp": sibling}
-        )
+        ref = full(w, rank)
+        return remote(ref, ref, s_send.at[w, 0], s_recv.at[w, 0], {"dp": sibling})
 
     def s_copy(w, k, second):
         ref = part(w, origin(k), 1 - side if second else side)
         slot = 1 + 2 * k + second
         return remote(ref, ref, s_send.at[w, slot], s_recv.at[w, slot], {"dp": sibling})
-
-    def local_copy(w):
-        return pltpu.make_async_copy(shards[w], full(w, rank), local_sem.at[w])
 
     def pass_y(w):
         for k in range(peers):
@@ -160,11 +186,33 @@
             {"sp": lax.rem(me + 1, n)},
         )
 
+    def extra_copy(offset):
+        return remote(
+            raw_ref.at[me],
+            raw_ref.at[me],
+            e_send.at[offset - 1],
+            e_recv.at[offset - 1],
+            {"sp": lax.rem(me + offset, n)},
+        )
+
     for w in range(5):
+        local_copy(w).wait()
         for k in range(peers):
             y_copy(w, k).start()
         s_own(w).start()
-        local_copy(w).start()
+    for copy in small:
+        copy.wait()
+    for offset in range(1, n):
+        extra_copy(offset).start()
+    for j in range(own):
+        init_ref[j] = start_ref[j].T.astype(jnp.bfloat16)
+
+    def norm_rows(s, carry):
+        rows = pl.ds(pl.multiple_of(s * length, length), length)
+        normed[rows, :] = rms_scale(tokens_ref[s], pre_ref[...]).astype(jnp.bfloat16)
+        return carry
+
+    lax.fori_loop(0, seqs, norm_rows, 0)
 
     @pl.when(me > 0)
     def _():
@@ -175,12 +223,32 @@
     def _():
         rbuf[0:own] = init_ref[...]
 
-    def norm_rows(s, carry):
-        rows = pl.ds(pl.multiple_of(s * length, length), length)
-        normed[rows, :] = rms_scale(tokens_ref[s], pre_ref[...]).astype(jnp.bfloat16)
+    gap = 1.0 - bound_ref[...]
+    row = lax.broadcasted_iota(jnp.int32, (length, length), 0)
+    col = lax.broadcasted_iota(jnp.int32, (length, length), 1)
+    causal = row >= col
+    ones = causal.astype(jnp.float32)
+    nt = (((1,), (1,)), ((), ()))
+    tn = (((0,), (0,)), ((), ()))
+    place = (length, n * length)
+    chosen = (
+        lax.broadcasted_iota(jnp.int32, place, 1)
+        == lax.broadcasted_iota(jnp.int32, place, 0) + me * length
+    ).astype(jnp.float32)
+    for offset in range(1, n):
+        extra_copy(offset).wait_recv()
+
+    def pick(i, carry):
+        extra_ref[i] = lax.dot_general(
+            chosen,
+            raw_ref[i],
+            nt,
+            precision=lax.Precision.HIGHEST,
+            preferred_element_type=jnp.float32,
+        )
         return carry
 
-    lax.fori_loop(0, seqs, norm_rows, 0)
+    lax.fori_loop(0, n, pick, 0)
 
     def project(w, dest, at, j):
         lanes = pl.ds(pl.multiple_of(j * tile, tile), tile)
@@ -196,8 +264,6 @@
 
         lax.fori_loop(0, cols // tile, step, 0)
 
-    for w in range(5):
-        local_copy(w).wait()
     pass_y(0)
     pass_y(1)
     pass_x(0)
@@ -207,26 +273,21 @@
     pass_y(2)
     arrived(1)
     project_all(1, f_v_ref, cols)
-    pass_x(2)
-    pass_y(3)
-    pass_x(3)
-    pass_y(4)
-
-    row = lax.broadcasted_iota(jnp.int32, (length, length), 0)
-    col = lax.broadcasted_iota(jnp.int32, (length, length), 1)
-    causal = row >= col
-    ones = causal.astype(jnp.float32)
-    nt = (((1,), (1,)), ((), ()))
-    tn = (((0,), (0,)), ((), ()))
     tiles = cols // tile
 
     def forward(s, carry):
         rows = pl.ds(pl.multiple_of(s * length, length), length)
         f_pre = f_v_ref[rows, 0:cols].astype(jnp.float32)
-        keys = gap_ref[...] * jax.nn.sigmoid(-f_pre)
-        extra = extra_ref[s]
+        keys = gap * jax.nn.sigmoid(-f_pre)
         spread = jnp.concatenate(
-            [jnp.broadcast_to(extra[:, h : h + 1], (length, hk)) for h in range(heads)], axis=1
+            [
+                jnp.broadcast_to(
+                    extra_ref[s * (heads // own) + h // own][:, h % own : h % own + 1],
+                    (length, hk),
+                )
+                for h in range(heads)
+            ],
+            axis=1,
         )
         decay = jnp.log1p(-keys) + spread
         cum = jnp.dot(
@@ -263,24 +324,37 @@
 
         @pl.when(s == 0)
         def _():
+            pass_x(2)
+            pass_y(3)
+
+        @pl.when(s == tiles)
+        def _():
             arrived(2)
 
-        @pl.when(s == tiles)
+        @pl.when(s == 2 * tiles - 1)
+        def _():
+            pass_x(3)
+            pass_y(4)
+
+        @pl.when(s == 2 * tiles)
         def _():
             arrived(3)
 
-        @pl.when(s < tiles)
-        def _():
-            project(2, q_g_ref, 0, s)
+        @pl.when(s == 3 * tiles)
+        def _():
+            pass_x(4)
 
         @pl.when(jnp.logical_and(s >= tiles, s < 2 * tiles))
         def _():
-            project(3, q_g_ref, cols, s - tiles)
+            project(2, q_g_ref, 0, s - tiles)
+
+        @pl.when(jnp.logical_and(s >= 2 * tiles, s < 3 * tiles))
+        def _():
+            project(3, q_g_ref, cols, s - 2 * tiles)
 
         return carry
 
     lax.fori_loop(0, seqs, forward, 0)
-    pass_x(4)
 
     def outputs(s, carry):
         rows = pl.ds(pl.multiple_of(s * length, length), length)
@@ -310,6 +384,8 @@
 
     lax.fori_loop(0, seqs, outputs, 0)
     arrived(4)
+    for offset in range(1, n):
+        extra_copy(offset).wait_send()
     for w in range(5):
         s_own(w).wait_send()
         for k in range(peers):
@@ -332,8 +408,8 @@
         lax.fori_loop(0, items, done, 0)
 
 
-def layer(tokens, pre, weights, extra, gap, init, gain, n, ways):
-    own, hv, hk = init.shape
+def layer(tokens, pre, weights, extra, bound, init, gain, n, ways):
+    own, hk, hv = init.shape
     seqs, length, width = tokens.shape
     items = own * n
     heads = items // seqs
@@ -351,10 +427,18 @@
             jax.ShapeDtypeStruct((rows, heads * hv), jnp.bfloat16),
             jax.ShapeDtypeStruct(whole(weights[4]), jnp.bfloat16),
         ],
-        in_specs=[vmem] * 11,
+        in_specs=[pl.BlockSpec(memory_space=pltpu.HBM)] * 11,
         out_specs=[vmem] * 2,
         scratch_shapes=[pltpu.VMEM(whole(w), jnp.bfloat16) for w in weights[:4]]
         + [
+            pltpu.VMEM(tokens.shape, jnp.bfloat16),
+            pltpu.VMEM(pre.shape, jnp.float32),
+            pltpu.VMEM((n,) + extra.shape, jnp.float32),
+            pltpu.VMEM((n, length, own), jnp.float32),
+            pltpu.VMEM(bound.shape, jnp.float32),
+            pltpu.VMEM(init.shape, jnp.float32),
+            pltpu.VMEM((own, hv, hk), jnp.bfloat16),
+            pltpu.VMEM(gain.shape, jnp.float32),
             pltpu.VMEM((rows, width), jnp.bfloat16),
             pltpu.VMEM((rows, heads * (hk + hv)), jnp.bfloat16),
             pltpu.VMEM((rows, heads * (hk + hv)), jnp.bfloat16),
@@ -371,7 +455,9 @@
             dma((5, peers)),
             dma((5, 1 + 2 * peers)),
             dma((5, 1 + 2 * peers)),
-            dma((5,)),
+            dma((11,)),
+            dma((n - 1,)),
+            dma((n - 1,)),
         ],
         compiler_params=pltpu.CompilerParams(
             collective_id=0, has_side_effects=True, vmem_limit_bytes=48 * 1024 * 1024
@@ -379,7 +465,7 @@
         cost_estimate=pl.CostEstimate(
             flops=6 * 10**9, bytes_accessed=2 * 10**7, transcendentals=10**6
         ),
-    )(tokens, pre, *weights, extra, gap, init, gain)
+    )(tokens, pre, *weights, extra, bound, init, gain)
 
 
 def body(
@@ -399,17 +485,13 @@
     post_gain,
 ):
     seq_count, local_len, width = tokens.shape
-    heads = w_query.shape[1] // initial_state.shape[1]
-    extra = lax.all_to_all(extra_decay, "sp", split_axis=1, concat_axis=0, tiled=True)
-    extra = extra.reshape(seq_count, heads, local_len).transpose(0, 2, 1)
-    init = jnp.swapaxes(initial_state, 1, 2).astype(jnp.bfloat16)
     gated, w_o = layer(
         tokens,
         pre_gain[None, :],
         (w_forget, w_value, w_query, w_gate, w_out),
-        extra,
-        (1.0 - lower_bound)[None, :],
-        init,
+        extra_decay,
+        lower_bound[None, :],
+        initial_state,
         norm_gain[None, :],
         n,
         ways,

time: 119 us -> 111 us (0.933)
  starting transfers between devices: 6 us -> 0 us
  other arithmetic: 3.09 us -> 1.74 us
    all_to_all x1 -> x0, starting transfers between devices: 6 us -> none  [body(): lax.all_to_all(extra_decay, 'sp', split_axis=1, concat_axis=0, tiled=True)]
    all_to_all x4 -> x0, local copies, waits for them, and re-layouts: 1.44 us -> none  [body(): lax.all_to_all(extra_decay, 'sp', split_axis=1, concat_axis=0, tiled=True)]
    unnamed x19 -> x22, local copies, waits for them, and re-layouts: 8.39 us -> 8.89 us
  transfers between devices with their start and end apart: 1 -> 0, of which waited for: 1 -> 0; matrix products, arithmetic and copies ran while one was open for 1% -> 0% of each run, Pallas kernels for 0% -> 0%
where the time goes in v3:
time: 111 us; the launch traced here: 110 us
  Pallas kernels  98.3 us (89%)
  local copies, waits for them, and re-layouts  8.89 us (8%)
  other arithmetic  1.74 us (2%)
  matrix products  1.35 us (1%)
    pallas_call x1, Pallas kernels, layer(): pl.pallas_call(functools.partial(layer_kernel, n, ways, heads), out_shape...  98.3 us
    unnamed x22, local copies, waits for them, and re-layouts  8.89 us

profile of v3, /device:TPU:26, one launch (start us, length us, event | category | flops | bytes accessed | tf_op | source)
XLA Modules:
  0.0 110.4 jit_solution(15108138324984087710)
XLA Ops:
  0.0 0.0 copy-start
  0.0 1.0 copy-done
  1.0 0.0 copy-start.1
  1.0 1.0 copy-done.1
  2.1 0.0 copy-start.2
  2.1 1.0 copy-done.2
  3.1 0.0 copy-start.3
  3.1 1.0 copy-done.3
  4.2 0.0 copy-start.4
  4.2 1.0 copy-done.4
  5.2 0.0 copy-start.5
  5.2 0.9 copy-done.5
  6.2 0.0 copy-start.6
  6.2 0.7 copy-done.6
  6.9 0.0 copy-start.7
  6.9 0.7 copy-done.7
  7.6 0.0 copy-start.8
  7.6 0.7 copy-done.8
  8.2 0.0 copy-start.9
  8.2 0.7 copy-done.9
  8.9 98.3 %shard_map.118 = (bf16[512,512]{1,0:T(8,128)(2,1)S(1)}, bf16[512,2048]{1,0:T(8,128)(2,1)S(1)}) custom-call(bf16[8,64,2048]{2,1,0:T(8,128)(2,1)} %tokens_hbm.1, f32[1,2048]{1,0:T(1,128)S(1)} %bitcast.6, bf16[512,512]{1,0:T(8,128)(2,1)S(1)} %copy-done, bf16[512,512]{1,0:T(8,128)(2,1)S(1)} %copy-done.1, bf16[512,512]{1,0:T(8,128)(2,1)S(1)} %copy-done.2, ...), custom_call_target="tpu_custom_call" | custom-call | flops 6000000000 | bytes 20000000 | tf_op jit(solution)/shard_map/pallas_call | solution.py:424
  107.3 0.0 copy-start.10
  107.3 1.3 %multiply_reduce_fusion = (f32[512]{0:T(512)S(1)}, f32[512,2048]{1,0:T(8,128)S(1)}) fusion(bf16[512,512]{1,0:T(8,128)(2,1)S(1)} %get-tuple-element.7, bf16[512,2048]{1,0:T(8,128)(2,1)S(1)} %get-tuple-element.8), kind=kOutput, calls=%fused_computation.1 | convolution fusion | flops 1075838464 | bytes 6817792 | tf_op jit(solution)/shard_map/dot_general | solution.py:499
  108.6 0.0 copy-done.10
  108.6 1.7 %multiply_convert_fusion = bf16[512,2048]{1,0:T(8,128)(2,1)} fusion(f32[512,2048]{1,0:T(8,128)S(1)} %get-tuple-element.10, f32[2048]{0:T(1024)S(1)} %copy-done.10, f32[512]{0:T(512)S(1)} %add_rsqrt_fusion), kind=kLoop, calls=%fused_computation | loop fusion | flops 3145728 | bytes 6301696 | tf_op jit(solution)/shard_map/convert_element_type | solution.py:500
  (1 shorter events, 0.0 us)
Async XLA Ops:
  0.0 1.0 copy-start
  1.0 1.0 copy-start.1
  2.1 1.0 copy-start.2
  3.1 1.0 copy-start.3
  4.2 1.0 copy-start.4
  5.2 0.9 copy-start.5
  6.2 0.7 copy-start.6
  6.9 0.7 copy-start.7
  7.6 0.7 copy-start.8
  8.2 0.7 copy-start.9
  107.3 1.4 %copy-start.10 = (f32[2048]{0:T(1024)S(1)}, f32[2048]{0:T(1024)}, u32[]{:S(2)}) copy-start(f32[2048]{0:T(1024)} %param.23) | copy-start | bytes 24580
